TPU v7x, 32 devices: a whole 2x2x4 slice. The times are simulated.
32 devices in a mesh: grp: 2 (over y), kv: 4 (over z), tp: 4 (over x, core).
Axes of the slice: x: 2, y: 2, z: 4, core: 2. Of those that a mesh axis runs over, the one named last changes fastest.
Arguments:
- stream: bfloat16 [16, 4096], P('grp', 'kv'), parts along dimension 0, may hold values from -6 to 6
- attn_gain: bfloat16 [4096], P('kv'), may hold values from 0.099609375 to 1.8984375
- query_weight: bfloat16 [4096, 4096], P('kv', 'tp'), may hold values from -0.09375 to 0.09375
- query_gain: float32 [64], replicated, may hold values from 0.1 to 1.9
- key_cache: bfloat16 [16, 2048, 1024], P('grp', 'kv', 'tp'), parts along dimension 0, may hold values from -200 to 200
- value_cache: bfloat16 [16, 2048, 1024], P('grp', 'kv', 'tp'), parts along dimension 0, may hold values from -6 to 6
- gate_cache: float32 [16, 16, 2048], P('grp', 'tp', 'kv'), parts along dimension 0, may hold values from -2048 to 0, as said below
- output_weight: bfloat16 [4096, 4096], P('tp', 'kv'), may hold values from -0.75 to 0.75
- mixer_gain: bfloat16 [4096], replicated, may hold values from 0.099609375 to 1.8984375
- up_weight: bfloat16 [16384, 4096], P(('kv', 'tp')), may hold values from -0.09375 to 0.09375
- down_weight: bfloat16 [16384, 4096], P(('kv', 'tp')), may hold values from -0.0625 to 0.0625
Outputs:
- result: bfloat16 [16, 4096], P('grp', ('kv', 'tp')), parts along dimension 0
There are 2 independent parts, one for each index of `grp`. A program takes and returns all parts, laid end to end along the dimension named above; an argument that names none is the same for every part. Nothing has to cross between parts.
Inputs may be any that keep to these rules, and one draw needn't show every extreme that they name: `gate_cache`: cumulative log forget gates: along positions each row never rises.
All inputs are finite; a program needn't handle non-finite values.
Results may differ from a plain program's by a relative error of at most 0.007.
The roundings to bfloat16 on the way count: a program that leaves them out, or rounds other values in their place, can miss the bound.
Values may be sent and summed in bfloat16 or wider, within the bound.
No kernel may reach another device: no remote copies, remote signals or barrier semaphores. Data moves between devices by JAX's collectives and lax.ppermute only.
A program may use at most 64 MiB of HBM per device.

v0:
```python
import jax
import jax.numpy as jnp
from jax import lax
from jax.sharding import PartitionSpec as P

HEAD_DIM = 64


EPS = 1e-06


def rms_scale(values):
    return lax.rsqrt(jnp.mean(values * values, axis=-1, keepdims=True) + EPS)


def block_attention(queries, key_block, value_block, gate_block):
    batch_rows, position_index = (key_block.shape[0], key_block.shape[1])
    kv_local = queries.shape[1]
    key_heads = key_block.reshape(batch_rows, position_index, kv_local, HEAD_DIM)
    value_heads = value_block.reshape(batch_rows, position_index, kv_local, HEAD_DIM)
    scores = jnp.einsum("skgd,spkd->skgp", queries, key_heads, preferred_element_type=jnp.float32)
    scores = scores * HEAD_DIM ** (-0.5) - gate_block[:, :, None, :]
    score_top = jnp.max(scores, axis=-1)
    weights_exp = jnp.exp(scores - score_top[..., None])
    totals = jnp.sum(weights_exp, axis=-1)
    weighted = jnp.einsum(
        "skgp,spkd->skgd",
        weights_exp.astype(jnp.bfloat16),
        value_heads,
        preferred_element_type=jnp.float32,
    )
    return (score_top, totals, weighted)


def per_device(
    stream,
    attn_gain,
    query_weight,
    query_gain,
    key_cache,
    value_cache,
    gate_cache,
    output_weight,
    mixer_gain,
    up_weight,
    down_weight,
):
    batch_rows = stream.shape[0]
    scaled = (stream.astype(jnp.float32) * attn_gain.astype(jnp.float32)).astype(jnp.bfloat16)
    partial_value = jnp.dot(scaled, query_weight, preferred_element_type=jnp.float32)
    query_raw = lax.psum(partial_value, "kv")
    kv_local = key_cache.shape[2] // HEAD_DIM
    heads_local = query_raw.shape[1] // HEAD_DIM
    query_heads = query_raw.reshape(batch_rows, heads_local, HEAD_DIM)
    queries = (query_heads * rms_scale(query_heads) * query_gain).astype(jnp.bfloat16)
    queries = queries.reshape(batch_rows, kv_local, heads_local // kv_local, HEAD_DIM)
    score_top, totals, weighted = block_attention(queries, key_cache, value_cache, gate_cache)
    best = lax.pmax(score_top, "kv")
    factor = jnp.exp(score_top - best)
    totals, weighted = lax.psum((factor * totals, factor[..., None] * weighted), "kv")
    attended = (weighted / totals[..., None]).reshape(batch_rows, heads_local * HEAD_DIM)
    attended = attended.astype(jnp.bfloat16)
    projected = jnp.dot(attended, output_weight, preferred_element_type=jnp.float32)
    projected = lax.psum_scatter(projected, "tp", scatter_dimension=1, tiled=True)
    slice_width = projected.shape[1]
    own_slice = lax.dynamic_slice_in_dim(stream, lax.axis_index("tp") * slice_width, slice_width, 1)
    residual = (own_slice.astype(jnp.float32) + projected).astype(jnp.bfloat16)
    full_rows = lax.all_gather(residual, ("kv", "tp"), axis=1, tiled=True).astype(jnp.float32)
    normed = (full_rows * rms_scale(full_rows) * mixer_gain.astype(jnp.float32)).astype(
        jnp.bfloat16
    )
    up_proj = lax.dot_general(
        normed, up_weight, (((1,), (1,)), ((), ())), preferred_element_type=jnp.float32
    )
    squared = jnp.square(jax.nn.relu(up_proj)).astype(jnp.bfloat16)
    partials = jnp.dot(squared, down_weight, preferred_element_type=jnp.float32)
    summed = lax.psum_scatter(partials, ("kv", "tp"), scatter_dimension=1, tiled=True)
    return (residual.astype(jnp.float32) + summed).astype(jnp.bfloat16)


def solution(mesh):
    in_specs = (
        P("grp", "kv"),
        P("kv"),
        P("kv", "tp"),
        P(),
        P("grp", "kv", "tp"),
        P("grp", "kv", "tp"),
        P("grp", "tp", "kv"),
        P("tp", "kv"),
        P(),
        P(("kv", "tp"), None),
        P(("kv", "tp"), None),
    )
    out_specs = P("grp", ("kv", "tp"))
    return jax.shard_map(
        per_device, mesh=mesh, in_specs=in_specs, out_specs=out_specs, check_vma=False
    )
```

profile of v0, /device:TPU:0, one launch (start us, length us, event | category | flops | bytes accessed | tf_op | source)
XLA Modules:
  0.0 189.7 jit_solution(11805961911175229180)
XLA Ops:
  6.5 0.0 copy-start
  6.5 0.0 reduce-scatter.3.cloned.1.call-start
  6.5 0.8 convert_element_type.48
  7.4 0.8 copy-done
  8.1 1.1 fusion.19
  9.2 20.8 %psum.21 = f32[8,1024]{1,0:T(8,128)S(1)} all-reduce(f32[8,1024]{1,0:T(8,128)S(1)} %fusion.19), channel_id=1, replica_groups=mesh['grp'=2,'kv'=4,'tp'=4] {'kv'}, use_global_device_ids=true, to_apply=%region_0.0 | all-reduce | flops 8192 | bytes 65536 | tf_op jit(solution)/shard_map/psum | solution.py:51
  30.1 0.1 reshape.45
  30.2 0.1 mul.75
  30.2 0.1 reduce_sum.27
  30.4 0.1 copy.18
  30.4 0.1 copy.19
  30.5 0.0 copy-start.1
  30.5 0.0 copy-start.3
  30.5 4.0 %copy.20 = bf16[8,512,256]{1,2,0:T(8,128)(2,1)} copy(bf16[8,512,256]{2,1,0:T(8,128)(2,1)} %param.15) | data formatting | bytes 4194304 | tf_op args[4]
  34.5 0.0 copy-done.1
  34.5 0.0 copy-done.3
  34.5 2.1 %fusion.24 = (f32[8,4,4]{2,1,0:T(4,128)S(1)}, f32[8,4,4,512]{3,2,1,0:T(4,128)S(1)}) fusion(f32[8,4,512]{2,1,0:T(4,128)S(1)} %copy-done.1, bf16[8,512,4,64]{1,3,2,0:T(8,128)(2,1)} %bitcast.15, f32[8,4,4,64]{3,2,1,0:T(4,128)S(1)} %reshape.45, f32[64]{0:T(128)S(1)} %copy-done.3, f32[8,4,4]{2,1,0:T(4,128)S(1)} %copy.19), kind=kOutput, calls=%fused_computation.33 | convolution fusion | flops 8609664 | bytes 2458880 | tf_op jit(solution)/shard_map/skgd,spkd->skgp/dot_general | solution.py:21
  36.6 15.5 %pmax.7 = f32[8,4,4]{2,1,0:T(4,128)S(1)} all-reduce(f32[8,4,4]{2,1,0:T(4,128)S(1)} %get-tuple-element.9), channel_id=1, replica_groups=mesh['grp'=2,'kv'=4,'tp'=4] {'kv'}, use_global_device_ids=true, to_apply=%region_3.0 | all-reduce | flops 128 | bytes 1024 | tf_op jit(solution)/shard_map/pmax | solution.py:58
  52.2 0.2 fusion.4
  52.4 3.9 %copy.21 = bf16[8,512,256]{1,2,0:T(8,128)(2,1)} copy(bf16[8,512,256]{2,1,0:T(8,128)(2,1)} %param.16) | data formatting | bytes 4194304 | tf_op args[5]
  56.4 0.0 copy-start.2
  56.4 2.3 %convolution_multiply_fusion.1 = f32[8,4,4,64]{3,2,1,0:T(4,128)S(1)} fusion(bf16[8,512,4,64]{1,3,2,0:T(8,128)(2,1)} %bitcast.16, f32[8,4,4,512]{3,2,1,0:T(4,128)S(1)} %get-tuple-element.10, f32[8,4,4]{2,1,0:T(4,128)S(1)} %get-tuple-element.9, f32[8,4,4]{2,1,0:T(4,128)S(1)} %bitcast.22), kind=kOutput, calls=%fused_computation.2 | convolution fusion | flops 8527872 | bytes 2393088 | tf_op jit(solution)/shard_map/skgp,spkd->skgd/dot_general | solution.py:26
  58.7 17.6 %all-reduce = (f32[8,4,4,64]{3,2,1,0:T(4,128)S(1)}, f32[8,4,4]{2,1,0:T(4,128)S(1)}) all-reduce(f32[8,4,4,64]{3,2,1,0:T(4,128)S(1)} %convolution_multiply_fusion.1, f32[8,4,4]{2,1,0:T(4,128)S(1)} %bitcast.18), channel_id=1, replica_groups=mesh['grp'=2,'kv'=4,'tp'=4] {'kv'}, use_global_device_ids=true, to_apply=%region_4.0 | all-reduce | flops 8320 | bytes 66560 | tf_op jit(solution)/shard_map/psum | solution.py:60
  76.3 0.1 divide_convert_fusion
  76.4 0.1 convert_element_type.53
  76.5 2.6 %fusion.25 = f32[8,1024]{1,0:T(8,128)} fusion(bf16[8,1024]{1,0:T(8,128)(2,1)S(1)} %convert_element_type.53, bf16[1024,1024]{1,0:T(8,128)(2,1)} %param.18), kind=kOutput, calls=%fused_computation.34 | convolution fusion | flops 16777216 | bytes 2146304 | tf_op jit(solution)/shard_map/dot_general | solution.py:63
  79.1 0.0 reduce-scatter.3.cloned.1.call-update
  79.1 0.0 reduce-scatter.5.cloned.1.call-start
  79.1 0.0 copy-done.2
  79.2 18.2 %reduce-scatter.3.cloned.1.call-done = f32[8,256]{1,0:T(8,128)} async-done(((f32[8,1024]{1,0:T(8,128)}), f32[8,256]{1,0:T(8,128)}) %reduce-scatter.3.cloned.1.call-update) | async-done | bytes 8208 | tf_op jit(solution)/shard_map/reduce_scatter | solution.py:64
  97.4 0.7 add_convert_fusion.1
  98.1 20.6 %all_gather.3 = bf16[8,4096]{1,0:T(8,128)(2,1)S(1)} all-gather(bf16[8,256]{1,0:T(8,128)(2,1)S(1)} %add_convert_fusion.1), channel_id=1, replica_groups=mesh['grp'=2,'kv'=4,'tp'=4] {'kv','tp'}, dimensions={1}, use_global_device_ids=true | all-gather | bytes 69632 | tf_op jit(solution)/shard_map/all_gather | solution.py:68
  118.7 0.1 fusion.6
  118.8 9.8 %fusion.3 = f32[8,4096]{1,0:T(8,128)} fusion(bf16[1024,4096]{1,0:T(8,128)(2,1)} %param.21, bf16[1024,4096]{1,0:T(8,128)(2,1)} %param.20, bf16[8,4096]{1,0:T(8,128)(2,1)S(1)} %all_gather.3, f32[4096]{0:T(1024)S(1)} %convert_element_type.57, f32[8]{0:T(128)S(1)} %add_rsqrt_fusion.1), kind=kOutput, calls=%fused_computation.6 | convolution fusion | flops 134373376 | bytes 16990240 | tf_op jit(solution)/shard_map/dot_general | solution.py:76
  128.6 0.0 reduce-scatter.5.cloned.1.call-update
  128.6 53.0 %reduce-scatter.5.cloned.1.call-done = f32[8,256]{1,0:T(8,128)} async-done(((f32[8,4096]{1,0:T(8,128)}), f32[8,256]{1,0:T(8,128)}) %reduce-scatter.5.cloned.1.call-update) | async-done | bytes 8208 | tf_op jit(solution)/shard_map/reduce_scatter | solution.py:77
  181.6 1.3 add_convert_fusion
  (5 shorter events, 0.0 us)
Async XLA Ops:
  6.5 1.6 copy-start
  6.5 90.9 %reduce-scatter.3.cloned.1.call-start = ((), (), s32[]{:S(2)}) async-start(), calls=%async_computation.2 | async-start | bytes 40960 | tf_op jit(solution)/shard_map/reduce_scatter | solution.py:64
  30.5 4.0 %copy-start.1 = (f32[8,4,512]{2,1,0:T(4,128)S(1)}, f32[8,4,512]{2,1,0:T(4,128)}, u32[]{:S(2)}) copy-start(f32[8,4,512]{2,1,0:T(4,128)} %param.17) | copy-start | bytes 196612
  30.5 4.0 %copy-start.3 = (f32[64]{0:T(128)S(1)}, f32[64]{0:T(128)}, u32[]{:S(2)}) copy-start(f32[64]{0:T(128)} %param.14) | copy-start | bytes 772
  56.4 22.8 %copy-start.2 = (bf16[4096]{0:T(1024)(128)(2,1)S(1)}, bf16[4096]{0:T(1024)(128)(2,1)}, u32[]{:S(2)}) copy-start(bf16[4096]{0:T(1024)(128)(2,1)} %param.19) | copy-start | bytes 24580
  79.1 102.5 %reduce-scatter.5.cloned.1.call-start = ((), (), s32[]{:S(2)}) async-start(), calls=%async_computation.3 | async-start | bytes 139264 | tf_op jit(solution)/shard_map/reduce_scatter | solution.py:77
Sparse Core Ops, SparseCore 0:
  79.2 18.1 reduce-scatter.2
  128.8 52.8 reduce-scatter.4
where the time goes:
time: 190 us
  blocking collectives  74.5 us (39%)
  waiting for transfers between devices  71.2 us (37%)
  matrix products  17.9 us (9%)
  between operations  13.5 us (7%)
  local copies, waits for them, and re-layouts  9.15 us (5%)
  other arithmetic  3.46 us (2%)
    reduce_scatter x1, waiting for transfers between devices, per_device(): lax.psum_scatter(partials, ('kv', 'tp'), scatter_dimension=1, tiled=True)  53 us
    psum x1, blocking collectives, per_device(): query_raw = lax.psum(partial_value, 'kv')  20.8 us
    all_gather x1, blocking collectives, per_device(): lax.all_gather(residual, ('kv', 'tp'), axis=1, tiled=True)  20.6 us
    reduce_scatter x1, waiting for transfers between devices, per_device(): lax.psum_scatter(projected, 'tp', scatter_dimension=1, tiled=True)  18.2 us
    psum x1, blocking collectives, per_device(): lax.psum((factor * totals, factor[..., None] * weighted), 'kv')  17.6 us
    pmax x1, blocking collectives, per_device(): best = lax.pmax(score_top, 'kv')  15.5 us
    dot_general x1, matrix products, per_device(): partials = jnp.dot(squared, down_weight, preferred_element_type=jnp.float32)  9.78 us
    unnamed x10, local copies, waits for them, and re-layouts  8.7 us
  transfers between devices with their start and end apart: 2, of which 2 were waited for; matrix products, arithmetic and copies ran while one was open for 0% of the time, Pallas kernels for 0%

commit v1 on v0

v1 whole, which is shorter than its diff:
```python
import functools

import jax
import jax.numpy as jnp
from jax import lax
from jax.experimental import pallas as pl
from jax.experimental.pallas import tpu as pltpu
from jax.sharding import PartitionSpec as P

HEAD_DIM = 64
EPS = 1e-06
LANES = 128
F32 = jnp.float32
BF16 = jnp.bfloat16
NT = (((1,), (1,)), ((), ()))
MIB = 1024 * 1024


def call(kernel, out_shape, args, scratch=(), limit=8):
    nbytes = sum(a.size * a.dtype.itemsize for a in args)
    return pl.pallas_call(
        kernel,
        out_shape=out_shape,
        in_specs=[pl.BlockSpec(memory_space=pltpu.VMEM)] * len(args),
        out_specs=pl.BlockSpec(memory_space=pltpu.VMEM),
        scratch_shapes=list(scratch),
        compiler_params=pltpu.CompilerParams(vmem_limit_bytes=limit * MIB),
        cost_estimate=pl.CostEstimate(flops=10**10, bytes_accessed=nbytes, transcendentals=0),
        name=kernel.__name__ if hasattr(kernel, "__name__") else kernel.func.__name__,
    )(*args)


def exchange(value, axis, size):
    return [
        lax.ppermute(value, axis, [(i, i ^ step) for i in range(size)])
        for step in range(1, size)
    ]


def tree_sum(terms):
    while len(terms) > 1:
        terms = [a + b for a, b in zip(terms[::2], terms[1::2])]
    return terms[0]


def query_kernel(stream_ref, gain_ref, weight_ref, out_ref):
    scaled = (stream_ref[...].astype(F32) * gain_ref[...].astype(F32)).astype(BF16)
    out_ref[...] = jnp.dot(scaled, weight_ref[...], preferred_element_type=F32)


def attention_kernel(count, kv_local, *refs):
    parts, (gain_ref, key_ref, value_ref, gate_ref, out_ref, wide_ref) = refs[:count], refs[count:]
    rows = out_ref.shape[0]
    width = kv_local * HEAD_DIM
    group = rows // key_ref.shape[0]
    heads = group * kv_local
    batch = key_ref.shape[0]
    raw = tree_sum([ref[...] for ref in parts])
    lane = lax.broadcasted_iota(jnp.int32, (batch, LANES), 1)
    low = lane < HEAD_DIM
    gain = jnp.concatenate([gain_ref[...]] * 2, axis=1)
    zero = jnp.zeros((batch, LANES), F32)
    for pair in range(heads // 2):
        vec = raw[:, pair * LANES : (pair + 1) * LANES]
        square = vec * vec
        sums = [
            jnp.sum(jnp.where(mask, square, 0.0), axis=1, keepdims=True)
            for mask in (low, jnp.logical_not(low))
        ]
        scales = [lax.rsqrt(s * (1.0 / HEAD_DIM) + EPS) for s in sums]
        query = (vec * jnp.where(low, scales[0], scales[1])) * gain
        swapped = pltpu.roll(query, HEAD_DIM, 1)
        for half in range(2):
            head = pair * 2 + half
            kv_head = head // group
            source = query if half == kv_head % 2 else swapped
            placed = jnp.where(low if kv_head % 2 == 0 else jnp.logical_not(low), source, 0.0)
            for column in range(width // LANES):
                block = placed if column == kv_head // 2 else zero
                wide_ref[column, head * batch : (head + 1) * batch, :] = block
    positions = key_ref.shape[1]
    head_row = lax.broadcasted_iota(jnp.int32, (heads, width), 0) // group
    own = head_row == lax.broadcasted_iota(jnp.int32, (heads, width), 1) // HEAD_DIM
    stat_row = lax.broadcasted_iota(jnp.int32, (heads, LANES), 0) // group
    stat_lane = lax.broadcasted_iota(jnp.int32, (heads, LANES), 1)
    for s in range(batch):
        query = jnp.concatenate(
            [
                wide_ref[column, pl.ds(s, heads, stride=batch), :]
                for column in range(width // LANES)
            ],
            axis=1,
        ).astype(BF16)
        scores = lax.dot_general(query, key_ref[s], NT, preferred_element_type=F32)
        gate = jnp.concatenate(
            [
                jnp.broadcast_to(gate_ref[s, k : k + 1, :], (group, positions))
                for k in range(kv_local)
            ],
            axis=0,
        )
        scores = scores * HEAD_DIM ** (-0.5) - gate
        top = jnp.max(scores, axis=1, keepdims=True)
        probs = jnp.exp(scores - top)
        total = jnp.sum(probs, axis=1, keepdims=True)
        weighted = jnp.dot(probs.astype(BF16), value_ref[s], preferred_element_type=F32)
        weighted = jnp.where(own, weighted, 0.0)
        stats = jnp.where(stat_lane == stat_row, top, 0.0)
        stats = stats + jnp.where(stat_lane == stat_row + kv_local, total, 0.0)
        row = jnp.concatenate([weighted, stats], axis=1)
        out_ref[s * group : (s + 1) * group, :] = tree_sum(
            [row[k * group : (k + 1) * group] for k in range(kv_local)]
        )


def project_kernel(count, kv_local, *refs):
    parts, (weight_ref, out_ref, attended_ref) = refs[:count], refs[count:]
    width = kv_local * HEAD_DIM
    rows = parts[0].shape[0]
    batch = out_ref.shape[0]
    group = rows // batch
    stats = [ref[:, width:] for ref in parts]
    best = functools.reduce(jnp.maximum, stats)
    factors = [jnp.exp(s - best) for s in stats]
    totals = sum(f * pltpu.roll(s, LANES - kv_local, 1) for f, s in zip(factors, stats))
    block = lax.broadcasted_iota(jnp.int32, (rows, width), 1) // HEAD_DIM

    def expand(narrow):
        wide = jnp.broadcast_to(narrow[:, 0:1], (rows, width))
        for k in range(1, kv_local):
            wide = jnp.where(block == k, narrow[:, k : k + 1], wide)
        return wide

    weighted = sum(expand(f) * ref[:, :width] for f, ref in zip(factors, parts))
    attended = weighted / expand(totals)
    for column in range(width // LANES):
        attended_ref[column] = attended[:, column * LANES : (column + 1) * LANES]
    acc = None
    for g in range(group):
        attended = jnp.concatenate(
            [
                attended_ref[column, pl.ds(g, batch, stride=group), :]
                for column in range(width // LANES)
            ],
            axis=1,
        ).astype(BF16)
        weight = jnp.concatenate(
            [
                weight_ref[(k * group + g) * HEAD_DIM : (k * group + g + 1) * HEAD_DIM, :]
                for k in range(kv_local)
            ],
            axis=0,
        )
        term = jnp.dot(attended, weight, preferred_element_type=F32)
        acc = term if acc is None else acc + term
    out_ref[...] = acc


def mixer_kernel(count, *refs):
    parts, (gain_ref, up_ref, down_ref, out_ref, rows_ref) = refs[:count], refs[count:]
    chunk = parts[0].shape[1]
    model = rows_ref.shape[1]
    index = lax.axis_index("kv") if count > 1 else 0
    for step, ref in enumerate(parts):
        start = pl.multiple_of(jnp.bitwise_xor(index, step) * chunk, LANES)
        rows_ref[:, pl.ds(start, chunk)] = ref[...].astype(F32)
    rows = rows_ref[...]
    scale = lax.rsqrt(jnp.mean(rows * rows, axis=1, keepdims=True) + EPS)
    normed = (rows * scale * gain_ref[...].astype(F32)).astype(BF16)
    hidden = up_ref.shape[0]
    tile = 256
    squared = []
    for start in range(0, hidden, tile):
        pre = lax.dot_general(
            up_ref[start : start + tile, :], normed, NT, preferred_element_type=F32
        )
        squared.append(jnp.square(jnp.maximum(pre, 0.0)).T.astype(BF16))
    squared = jnp.concatenate(squared, axis=1)
    blocks, _, width = out_ref.shape
    for b in range(blocks):
        out_ref[b] = jnp.dot(
            squared, down_ref[:, b * width : (b + 1) * width], preferred_element_type=F32
        ).astype(out_ref.dtype)


def per_device(
    kv_size,
    tp_size,
    stream,
    attn_gain,
    query_weight,
    query_gain,
    key_cache,
    value_cache,
    gate_cache,
    output_weight,
    mixer_gain,
    up_weight,
    down_weight,
):
    batch, chunk = stream.shape
    heads_width = query_weight.shape[1]
    kv_local = key_cache.shape[2] // HEAD_DIM
    heads_local = heads_width // HEAD_DIM
    group = heads_local // kv_local
    width = kv_local * HEAD_DIM

    def shape(dims, dtype):
        return jax.ShapeDtypeStruct(dims, dtype)

    partial = call(
        query_kernel,
        shape((batch, heads_width), F32),
        (stream, attn_gain[None], query_weight),
    )
    if kv_size <= 4:
        queries = [partial] + exchange(partial, "kv", kv_size)
    else:
        queries = [lax.psum(partial, "kv")]
    mine = call(
        functools.partial(attention_kernel, len(queries), kv_local),
        shape((batch * group, width + LANES), F32),
        (*queries, query_gain[None], key_cache, value_cache, gate_cache),
        scratch=[pltpu.VMEM((width // LANES, heads_local * batch, LANES), F32)],
    )
    if kv_size <= 4:
        blocks = [mine] + exchange(mine, "kv", kv_size)
    else:
        gathered = lax.all_gather(mine, "kv")
        blocks = [gathered[i] for i in range(kv_size)]
    projected = call(
        functools.partial(project_kernel, len(blocks), kv_local),
        shape((batch, output_weight.shape[1]), F32),
        (*blocks, output_weight),
        scratch=[pltpu.VMEM((width // LANES, batch * group, LANES), F32)],
    )
    if tp_size <= 4:
        projected = tree_sum([projected] + exchange(projected, "tp", tp_size))
    else:
        projected = lax.psum(projected, "tp")
    residual = (stream.astype(F32) + projected).astype(BF16)
    if kv_size <= 4:
        chunks = [residual] + exchange(residual, "kv", kv_size)
    else:
        chunks = [lax.all_gather(residual, "kv", axis=1, tiled=True)]
    devices = kv_size * tp_size
    model = down_weight.shape[1]
    own_width = model // devices
    partials = call(
        functools.partial(mixer_kernel, len(chunks)),
        shape((devices, batch, own_width), F32),
        (*chunks, mixer_gain[None], up_weight, down_weight),
        scratch=[pltpu.VMEM((batch, model), F32)],
        limit=20,
    )
    arrived = lax.all_to_all(partials, ("kv", "tp"), 0, 0)
    own = lax.dynamic_slice_in_dim(residual, lax.axis_index("tp") * own_width, own_width, 1)
    return (own.astype(F32) + jnp.sum(arrived, axis=0)).astype(BF16)


def solution(mesh):
    in_specs = (
        P("grp", "kv"),
        P("kv"),
        P("kv", "tp"),
        P(),
        P("grp", "kv", "tp"),
        P("grp", "kv", "tp"),
        P("grp", "tp", "kv"),
        P("tp", "kv"),
        P(),
        P(("kv", "tp"), None),
        P(("kv", "tp"), None),
    )
    out_specs = P("grp", ("kv", "tp"))
    return jax.shard_map(
        functools.partial(per_device, mesh.shape["kv"], mesh.shape["tp"]),
        mesh=mesh,
        in_specs=in_specs,
        out_specs=out_specs,
        check_vma=False,
    )
```

time: 190 us -> 54.1 us (0.28)
  blocking collectives: 74.5 us -> 0 us
  waiting for transfers between devices: 71.2 us -> 22.4 us
  starting transfers between devices: 0.04 us -> 19.6 us
  matrix products: 17.9 us -> 0 us
  between operations: 13.5 us -> 0.15 us
  Pallas kernels: 0 us -> 7.89 us
  local copies, waits for them, and re-layouts: 9.15 us -> 3.07 us
  other arithmetic: 3.46 us -> 0.64 us
    reduce_scatter x2 -> x0, waiting for transfers between devices: 71.2 us -> none  [the longest x1 53 us: per_device(): lax.psum_scatter(partials, ('kv', 'tp'), scatter_dimension=1, tiled=True)]
    psum x2 -> x0, blocking collectives: 38.4 us -> none  [the longest x1 20.8 us: per_device(): query_raw = lax.psum(partial_value, 'kv')]
    all_gather x1 -> x0, blocking collectives: 20.6 us -> none  [per_device(): lax.all_gather(residual, ('kv', 'tp'), axis=1, tiled=True)]
    dot_general x5 -> x0, matrix products: 17.9 us -> none  [the longest x1 9.78 us: per_device(): partials = jnp.dot(squared, down_weight, preferred_element_type=jnp.float32)]
    ppermute x0 -> x12, starting transfers between devices: none -> 15.9 us  [exchange(): lax.ppermute(value, axis, [(i, i ^ step) for i in range(size)])]
    pmax x1 -> x0, blocking collectives: 15.5 us -> none  [per_device(): best = lax.pmax(score_top, 'kv')]
    ppermute x0 -> x12, waiting for transfers between devices: none -> 14.5 us  [exchange(): lax.ppermute(value, axis, [(i, i ^ step) for i in range(size)])]
    all_to_all x0 -> x1, waiting for transfers between devices: none -> 7.9 us  [per_device(): arrived = lax.all_to_all(partials, ('kv', 'tp'), 0, 0)]
  transfers between devices with their start and end apart: 2 -> 13, of which waited for: 2 -> 11; matrix products, arithmetic and copies ran while one was open for 0% -> 0% of each run, Pallas kernels for 0% -> 0%
where the time goes in v1:
time: 54.1 us; the launch traced here: 53.7 us
  waiting for transfers between devices  22.4 us (41%)
  starting transfers between devices  19.6 us (36%)
  Pallas kernels  7.89 us (15%)
  local copies, waits for them, and re-layouts  3.07 us (6%)
  other arithmetic  0.64 us (1%)
    ppermute x12, starting transfers between devices, exchange(): lax.ppermute(value, axis, [(i, i ^ step) for i in range(size)])  15.9 us
    ppermute x12, waiting for transfers between devices, exchange(): lax.ppermute(value, axis, [(i, i ^ step) for i in range(size)])  14.5 us
    all_to_all x1, waiting for transfers between devices, per_device(): arrived = lax.all_to_all(partials, ('kv', 'tp'), 0, 0)  7.9 us
    pallas_call x4, Pallas kernels, call(): pl.pallas_call(kernel, out_shape=out_shape, in_specs=[pl.BlockSpec(memory...  7.89 us
    all_to_all x1, starting transfers between devices, per_device(): arrived = lax.all_to_all(partials, ('kv', 'tp'), 0, 0)  3.66 us
    unnamed x26, local copies, waits for them, and re-layouts  2.37 us
  transfers between devices with their start and end apart: 13, of which 11 were waited for; matrix products, arithmetic and copies ran while one was open for 0% of the time, Pallas kernels for 0%

profile of v1, /device:TPU:0, one launch (start us, length us, event | category | flops | bytes accessed | tf_op | source)
XLA Modules:
  0.0 53.7 jit_solution(2814842748524288013)
XLA Ops:
  0.0 0.7 %broadcast_in_dim.9.gain_ref = bf16[1,1024]{1,0:T(2,128)(2,1)S(1)} reshape(bf16[1024]{0:T(1024)(128)(2,1)} %param.12) | data formatting | bytes 4096 | tf_op jit(solution)/shard_map/broadcast_in_dim | solution.py:214
  0.7 0.0 copy-start
  0.7 0.7 %copy-done = bf16[8,1024]{1,0:T(8,128)(2,1)S(1)} copy-done((bf16[8,1024]{1,0:T(8,128)(2,1)S(1)}, bf16[8,1024]{1,0:T(8,128)(2,1)}, u32[]{:S(2)}) %copy-start) | copy-done | bytes 16408
  1.4 0.0 copy-start.2
  1.4 1.6 %copy-done.2 = bf16[1024,1024]{1,0:T(8,128)(2,1)S(1)} copy-done((bf16[1024,1024]{1,0:T(8,128)(2,1)S(1)}, bf16[1024,1024]{1,0:T(8,128)(2,1)}, u32[]{:S(2)}) %copy-start.2) | copy-done | bytes 2097176
  3.0 0.0 copy-start.3
  3.0 0.0 copy-start.4
  3.0 0.0 copy-start.6
  3.0 0.0 copy-start.7
  3.0 0.4 query_kernel.1.refs_0_
  3.4 3.1 %collective-permute-start = (f32[8,1024]{1,0:T(8,128)S(1)}, f32[8,1024]{1,0:T(8,128)S(1)}, u32[]{:S(2)}, u32[]{:S(2)}) collective-permute-start(f32[8,1024]{1,0:T(8,128)S(1)} %query_kernel.1.refs_0_), channel_id=1, source_target_pairs={{0,4},{4,0},{8,12},{12,8},{1,5},{5,1},{9,13},{13,9},{2,6},{6,2},{1... | collective-permute-start | bytes 98312 | tf_op jit(solution)/shard_map/ppermute | solution.py:35
  6.5 2.6 %collective-permute-start.1 = (f32[8,1024]{1,0:T(8,128)S(1)}, f32[8,1024]{1,0:T(8,128)S(1)}, u32[]{:S(2)}, u32[]{:S(2)}) collective-permute-start(f32[8,1024]{1,0:T(8,128)S(1)} %query_kernel.1.refs_0_), channel_id=1, source_target_pairs={{0,8},{4,12},{8,0},{12,4},{1,9},{5,13},{9,1},{13,5},{2,10},{6,14},... | collective-permute-start | bytes 98312 | tf_op jit(solution)/shard_map/ppermute | solution.py:35
  9.0 0.0 collective-permute-start.2
  9.0 0.0 collective-permute-done.refs_1_
  9.0 2.8 %collective-permute-done.1.refs_2_ = f32[8,1024]{1,0:T(8,128)S(1)} collective-permute-done((f32[8,1024]{1,0:T(8,128)S(1)}, f32[8,1024]{1,0:T(8,128)S(1)}, u32[]{:S(2)}, u32[]{:S(2)}) %collective-permute-start.1) | collective-permute-done | bytes 32800 | tf_op jit(solution)/shard_map/ppermute | solution.py:35
  11.8 2.9 %collective-permute-done.2.refs_3_ = f32[8,1024]{1,0:T(8,128)S(1)} collective-permute-done((f32[8,1024]{1,0:T(8,128)S(1)}, f32[8,1024]{1,0:T(8,128)S(1)}, u32[]{:S(2)}, u32[]{:S(2)}) %collective-permute-start.2) | collective-permute-done | bytes 32800 | tf_op jit(solution)/shard_map/ppermute | solution.py:35
  14.8 0.0 copy-done.3
  14.8 0.0 copy-done.4
  14.8 0.0 copy-done.6
  14.8 0.0 copy-done.7
  14.8 0.0 copy-start.5
  14.8 0.0 slice-start
  14.8 0.0 slice-start.2
  14.8 2.7 %attention_kernel.1.refs_0_ = f32[32,384]{1,0:T(8,128)S(1)} custom-call(f32[8,1024]{1,0:T(8,128)S(1)} %query_kernel.1.refs_0_, f32[8,1024]{1,0:T(8,128)S(1)} %collective-permute-done.refs_1_, f32[8,1024]{1,0:T(8,128)S(1)} %collective-permute-done.1.refs_2_, f32[8,1024]{1,0:T(8,128)S(1)} %collective-permute-done.2.refs_3_, f32[1,64]{1,0:T(1,128)S(1)} %bitcast.5, ...), custom_call_target="tpu_custom_call" | custom-call | flops 10000000000 | bytes 4391168 | tf_op jit(solution)/shard_map/attention_kernel/pallas_call | solution.py:21
  17.5 0.0 copy-start.1
  17.5 0.0 copy-start.8
  17.5 0.0 slice-start.1
  17.5 0.0 slice-start.3
  17.6 0.1 collective-permute-start.3
  17.6 0.9 %collective-permute-start.4 = (f32[32,384]{1,0:T(8,128)S(1)}, f32[32,384]{1,0:T(8,128)S(1)}, u32[]{:S(2)}, u32[]{:S(2)}) collective-permute-start(f32[32,384]{1,0:T(8,128)S(1)} %attention_kernel.1.refs_0_), channel_id=1, source_target_pairs={{0,8},{4,12},{8,0},{12,4},{1,9},{5,13},{9,1},{13,5},{2,10},{6,14},... | collective-permute-start | bytes 147464 | tf_op jit(solution)/shard_map/ppermute | solution.py:35
  18.5 3.5 %collective-permute-start.5 = (f32[32,384]{1,0:T(8,128)S(1)}, f32[32,384]{1,0:T(8,128)S(1)}, u32[]{:S(2)}, u32[]{:S(2)}) collective-permute-start(f32[32,384]{1,0:T(8,128)S(1)} %attention_kernel.1.refs_0_), channel_id=1, source_target_pairs={{0,12},{4,8},{8,4},{12,0},{1,13},{5,9},{9,5},{13,1},{2,14},{6,10},... | collective-permute-start | bytes 147464 | tf_op jit(solution)/shard_map/ppermute | solution.py:35
  22.0 0.1 collective-permute-done.3.refs_1_
  22.1 0.6 %collective-permute-done.4.refs_2_ = f32[32,384]{1,0:T(8,128)S(1)} collective-permute-done((f32[32,384]{1,0:T(8,128)S(1)}, f32[32,384]{1,0:T(8,128)S(1)}, u32[]{:S(2)}, u32[]{:S(2)}) %collective-permute-start.4) | collective-permute-done | bytes 49184 | tf_op jit(solution)/shard_map/ppermute | solution.py:35
  22.7 1.9 %collective-permute-done.5.refs_3_ = f32[32,384]{1,0:T(8,128)S(1)} collective-permute-done((f32[32,384]{1,0:T(8,128)S(1)}, f32[32,384]{1,0:T(8,128)S(1)}, u32[]{:S(2)}, u32[]{:S(2)}) %collective-permute-start.5) | collective-permute-done | bytes 49184 | tf_op jit(solution)/shard_map/ppermute | solution.py:35
  24.6 0.0 copy-done.5
  24.6 0.6 %project_kernel.1 = f32[8,1024]{1,0:T(8,128)S(1)} custom-call(f32[32,384]{1,0:T(8,128)S(1)} %attention_kernel.1.refs_0_, f32[32,384]{1,0:T(8,128)S(1)} %collective-permute-done.3.refs_1_, f32[32,384]{1,0:T(8,128)S(1)} %collective-permute-done.4.refs_2_, f32[32,384]{1,0:T(8,128)S(1)} %collective-permute-done.5.refs_3_, bf16[1024,1024]{1,0:T(8,128)(2,1)S(1)} %copy-done.5), custom_call_target="tpu_custom_call" | custom-call | flops 10000000000 | bytes 2293760 | tf_op jit(solution)/shard_map/project_kernel/pallas_call | solution.py:21
  25.2 0.0 collective-permute-start.6
  25.2 1.5 %collective-permute-start.7 = (f32[8,1024]{1,0:T(8,128)S(1)}, f32[8,1024]{1,0:T(8,128)S(1)}, u32[]{:S(2)}, u32[]{:S(2)}) collective-permute-start(f32[8,1024]{1,0:T(8,128)S(1)} %project_kernel.1), channel_id=1, source_target_pairs={{0,2},{1,3},{2,0},{3,1},{4,6},{5,7},{6,4},{7,5},{8,10},{9,11},{10,... | collective-permute-start | bytes 98312 | tf_op jit(solution)/shard_map/ppermute | solution.py:35
  26.7 0.3 collective-permute-start.8
  27.1 0.0 collective-permute-done.6
  27.1 2.1 %collective-permute-done.7 = f32[8,1024]{1,0:T(8,128)S(1)} collective-permute-done((f32[8,1024]{1,0:T(8,128)S(1)}, f32[8,1024]{1,0:T(8,128)S(1)}, u32[]{:S(2)}, u32[]{:S(2)}) %collective-permute-start.7) | collective-permute-done | bytes 32800 | tf_op jit(solution)/shard_map/ppermute | solution.py:35
  29.1 0.9 %collective-permute-done.8 = f32[8,1024]{1,0:T(8,128)S(1)} collective-permute-done((f32[8,1024]{1,0:T(8,128)S(1)}, f32[8,1024]{1,0:T(8,128)S(1)}, u32[]{:S(2)}, u32[]{:S(2)}) %collective-permute-start.8) | collective-permute-done | bytes 32800 | tf_op jit(solution)/shard_map/ppermute | solution.py:35
  30.1 0.0 copy-done.1
  30.1 0.2 collective-permute-start.10
  30.3 3.2 %collective-permute-start.11 = (bf16[8,1024]{1,0:T(8,128)(2,1)S(1)}, bf16[8,1024]{1,0:T(8,128)(2,1)S(1)}, u32[]{:S(2)}, u32[]{:S(2)}) collective-permute-start(bf16[8,1024]{1,0:T(8,128)(2,1)S(1)} %add_convert_fusion.refs_0_), channel_id=1, source_target_pairs={{0,12},{4,8},{8,4},{12,0},{1,13},{5,9},{9,5},{13,1},{2,14},{6,10},... | collective-permute-start | bytes 49160 | tf_op jit(solution)/shard_map/ppermute | solution.py:35
  33.5 0.5 collective-permute-start.9
  34.0 0.0 copy-done.8
  34.0 1.2 %collective-permute-done.10.refs_2_ = bf16[8,1024]{1,0:T(8,128)(2,1)S(1)} collective-permute-done((bf16[8,1024]{1,0:T(8,128)(2,1)S(1)}, bf16[8,1024]{1,0:T(8,128)(2,1)S(1)}, u32[]{:S(2)}, u32[]{:S(2)}) %collective-permute-start.10) | collective-permute-done | bytes 16416 | tf_op jit(solution)/shard_map/ppermute | solution.py:35
  35.2 0.6 %collective-permute-done.11.refs_3_ = bf16[8,1024]{1,0:T(8,128)(2,1)S(1)} collective-permute-done((bf16[8,1024]{1,0:T(8,128)(2,1)S(1)}, bf16[8,1024]{1,0:T(8,128)(2,1)S(1)}, u32[]{:S(2)}, u32[]{:S(2)}) %collective-permute-start.11) | collective-permute-done | bytes 16416 | tf_op jit(solution)/shard_map/ppermute | solution.py:35
  35.8 1.4 %collective-permute-done.9.refs_1_ = bf16[8,1024]{1,0:T(8,128)(2,1)S(1)} collective-permute-done((bf16[8,1024]{1,0:T(8,128)(2,1)S(1)}, bf16[8,1024]{1,0:T(8,128)(2,1)S(1)}, u32[]{:S(2)}, u32[]{:S(2)}) %collective-permute-start.9) | collective-permute-done | bytes 16416 | tf_op jit(solution)/shard_map/ppermute | solution.py:35
  37.3 0.0 slice-done
  37.3 0.0 slice-done.2
  37.3 0.0 slice-done.1
  37.3 0.0 slice-done.3
  37.3 4.2 %mixer_kernel.1 = f32[16,8,256]{2,1,0:T(8,128)} custom-call(bf16[8,1024]{1,0:T(8,128)(2,1)S(1)} %add_convert_fusion.refs_0_, bf16[8,1024]{1,0:T(8,128)(2,1)S(1)} %collective-permute-done.9.refs_1_, bf16[8,1024]{1,0:T(8,128)(2,1)S(1)} %collective-permute-done.10.refs_2_, bf16[8,1024]{1,0:T(8,128)(2,1)S(1)} %collective-permute-done.11.refs_3_, ...), custom_call_target="tpu_custom_call" | custom-call | flops 10000000000 | bytes 16850944 | tf_op jit(solution)/shard_map/mixer_kernel/pallas_call | solution.py:21
  41.5 3.7 %all-to-all-start = ((f32[16,8,256]{2,1,0:T(8,128)}), f32[16,8,256]{2,1,0:T(8,128)S(1)}, u32[]{:S(2)}, u32[]{:S(2)}) async-start(f32[16,8,256]{2,1,0:T(8,128)} %mixer_kernel.1), calls=%async_computation | async-start | bytes 262144 | tf_op jit(solution)/shard_map/all_to_all | solution.py:256
  45.2 7.9 %all-to-all-done = f32[16,8,256]{2,1,0:T(8,128)S(1)} async-done(((f32[16,8,256]{2,1,0:T(8,128)}), f32[16,8,256]{2,1,0:T(8,128)S(1)}, u32[]{:S(2)}, u32[]{:S(2)}) %all-to-all-start) | async-done | bytes 131104 | tf_op jit(solution)/shard_map/all_to_all | solution.py:256
  53.1 0.6 %add_convert_fusion.1 = bf16[8,256]{1,0:T(8,128)(2,1)} fusion(f32[8,256]{1,0:T(8,128)S(1)} %reduce_sum.9, bf16[8,1024]{1,0:T(8,128)(2,1)S(1)} %add_convert_fusion.refs_0_, s32[]{:T(128)S(6)} %select_n.3), kind=kLoop, calls=%fused_computation.1 | loop fusion | flops 6144 | bytes 16388 | tf_op jit(solution)/shard_map/convert_element_type | solution.py:258
  (5 shorter events, 0.0 us)
Async XLA Ops:
  0.7 0.7 %copy-start = (bf16[8,1024]{1,0:T(8,128)(2,1)S(1)}, bf16[8,1024]{1,0:T(8,128)(2,1)}, u32[]{:S(2)}) copy-start(bf16[8,1024]{1,0:T(8,128)(2,1)} %stream_ref.1) | copy-start | bytes 49156
  1.4 1.6 %copy-start.2 = (bf16[1024,1024]{1,0:T(8,128)(2,1)S(1)}, bf16[1024,1024]{1,0:T(8,128)(2,1)}, u32[]{:S(2)}) copy-start(bf16[1024,1024]{1,0:T(8,128)(2,1)} %weight_ref.1) | copy-start | bytes 6291460
  3.0 11.8 %copy-start.3 = (bf16[8,512,256]{2,1,0:T(8,128)(2,1)S(1)}, bf16[8,512,256]{2,1,0:T(8,128)(2,1)}, u32[]{:S(2)}) copy-start(bf16[8,512,256]{2,1,0:T(8,128)(2,1)} %refs_5_.2) | copy-start | bytes 6291460
  3.0 11.8 %copy-start.4 = (bf16[8,512,256]{2,1,0:T(8,128)(2,1)S(1)}, bf16[8,512,256]{2,1,0:T(8,128)(2,1)}, u32[]{:S(2)}) copy-start(bf16[8,512,256]{2,1,0:T(8,128)(2,1)} %refs_6_.2) | copy-start | bytes 6291460
  3.0 11.8 %copy-start.6 = (f32[8,4,512]{2,1,0:T(4,128)S(1)}, f32[8,4,512]{2,1,0:T(4,128)}, u32[]{:S(2)}) copy-start(f32[8,4,512]{2,1,0:T(4,128)} %refs_7_.1) | copy-start | bytes 196612
  3.0 11.8 %copy-start.7 = (f32[64]{0:T(128)S(1)}, f32[64]{0:T(128)}, u32[]{:S(2)}) copy-start(f32[64]{0:T(128)} %param.14) | copy-start | bytes 772
  3.4 5.7 %collective-permute-start = (f32[8,1024]{1,0:T(8,128)S(1)}, f32[8,1024]{1,0:T(8,128)S(1)}, u32[]{:S(2)}, u32[]{:S(2)}) collective-permute-start(f32[8,1024]{1,0:T(8,128)S(1)} %query_kernel.1.refs_0_), channel_id=1, source_target_pairs={{0,4},{4,0},{8,12},{12,8},{1,5},{5,1},{9,13},{13,9},{2,6},{6,2},{1... | collective-permute-start | bytes 98312 | tf_op jit(solution)/shard_map/ppermute | solution.py:35
  6.5 5.4 %collective-permute-start.1 = (f32[8,1024]{1,0:T(8,128)S(1)}, f32[8,1024]{1,0:T(8,128)S(1)}, u32[]{:S(2)}, u32[]{:S(2)}) collective-permute-start(f32[8,1024]{1,0:T(8,128)S(1)} %query_kernel.1.refs_0_), channel_id=1, source_target_pairs={{0,8},{4,12},{8,0},{12,4},{1,9},{5,13},{9,1},{13,5},{2,10},{6,14},... | collective-permute-start | bytes 98312 | tf_op jit(solution)/shard_map/ppermute | solution.py:35
  9.0 5.7 %collective-permute-start.2 = (f32[8,1024]{1,0:T(8,128)S(1)}, f32[8,1024]{1,0:T(8,128)S(1)}, u32[]{:S(2)}, u32[]{:S(2)}) collective-permute-start(f32[8,1024]{1,0:T(8,128)S(1)} %query_kernel.1.refs_0_), channel_id=1, source_target_pairs={{0,12},{4,8},{8,4},{12,0},{1,13},{5,9},{9,5},{13,1},{2,14},{6,10},... | collective-permute-start | bytes 98312 | tf_op jit(solution)/shard_map/ppermute | solution.py:35
  14.8 9.8 %copy-start.5 = (bf16[1024,1024]{1,0:T(8,128)(2,1)S(1)}, bf16[1024,1024]{1,0:T(8,128)(2,1)}, u32[]{:S(2)}) copy-start(bf16[1024,1024]{1,0:T(8,128)(2,1)} %refs_4_.1) | copy-start | bytes 6291460
  14.8 22.5 %slice-start = ((s8[8388608]{0:T(1024)(128)(4,1)}), s8[4194304]{0:T(1024)(128)(4,1)S(1)}, s32[]{:S(2)}) async-start(s8[8388608]{0:T(1024)(128)(4,1)} %bitcast.1), calls=%async_computation.1 | async-start | bytes 8388608
  14.8 22.5 %slice-start.2 = ((s8[8388608]{0:T(1024)(128)(4,1)}), s8[4194304]{0:T(1024)(128)(4,1)S(1)}, s32[]{:S(2)}) async-start(s8[8388608]{0:T(1024)(128)(4,1)} %bitcast.3), calls=%async_computation.3 | async-start | bytes 8388608
  17.5 12.6 %copy-start.1 = (bf16[8,1024]{1,0:T(8,128)(2,1)S(1)}, bf16[8,1024]{1,0:T(8,128)(2,1)}, u32[]{:S(2)}) copy-start(bf16[8,1024]{1,0:T(8,128)(2,1)} %stream_ref.1) | copy-start | bytes 49156
  17.5 16.5 %copy-start.8 = (bf16[4096]{0:T(1024)(128)(2,1)S(1)}, bf16[4096]{0:T(1024)(128)(2,1)}, u32[]{:S(2)}) copy-start(bf16[4096]{0:T(1024)(128)(2,1)} %param.19) | copy-start | bytes 24580
  17.5 19.7 %slice-start.1 = ((s8[8388608]{0:T(1024)(128)(4,1)}), s8[4194304]{0:T(1024)(128)(4,1)S(1)}, s32[]{:S(2)}) async-start(s8[8388608]{0:T(1024)(128)(4,1)} %bitcast.1), calls=%async_computation.2 | async-start | bytes 8388608
  17.5 19.7 %slice-start.3 = ((s8[8388608]{0:T(1024)(128)(4,1)}), s8[4194304]{0:T(1024)(128)(4,1)S(1)}, s32[]{:S(2)}) async-start(s8[8388608]{0:T(1024)(128)(4,1)} %bitcast.3), calls=%async_computation.4 | async-start | bytes 8388608
  17.6 4.5 %collective-permute-start.3 = (f32[32,384]{1,0:T(8,128)S(1)}, f32[32,384]{1,0:T(8,128)S(1)}, u32[]{:S(2)}, u32[]{:S(2)}) collective-permute-start(f32[32,384]{1,0:T(8,128)S(1)} %attention_kernel.1.refs_0_), channel_id=1, source_target_pairs={{0,4},{4,0},{8,12},{12,8},{1,5},{5,1},{9,13},{13,9},{2,6},{6,2},{1... | collective-permute-start | bytes 147464 | tf_op jit(solution)/shard_map/ppermute | solution.py:35
  17.6 5.1 %collective-permute-start.4 = (f32[32,384]{1,0:T(8,128)S(1)}, f32[32,384]{1,0:T(8,128)S(1)}, u32[]{:S(2)}, u32[]{:S(2)}) collective-permute-start(f32[32,384]{1,0:T(8,128)S(1)} %attention_kernel.1.refs_0_), channel_id=1, source_target_pairs={{0,8},{4,12},{8,0},{12,4},{1,9},{5,13},{9,1},{13,5},{2,10},{6,14},... | collective-permute-start | bytes 147464 | tf_op jit(solution)/shard_map/ppermute | solution.py:35
  18.5 6.1 %collective-permute-start.5 = (f32[32,384]{1,0:T(8,128)S(1)}, f32[32,384]{1,0:T(8,128)S(1)}, u32[]{:S(2)}, u32[]{:S(2)}) collective-permute-start(f32[32,384]{1,0:T(8,128)S(1)} %attention_kernel.1.refs_0_), channel_id=1, source_target_pairs={{0,12},{4,8},{8,4},{12,0},{1,13},{5,9},{9,5},{13,1},{2,14},{6,10},... | collective-permute-start | bytes 147464 | tf_op jit(solution)/shard_map/ppermute | solution.py:35
  25.2 1.9 %collective-permute-start.6 = (f32[8,1024]{1,0:T(8,128)S(1)}, f32[8,1024]{1,0:T(8,128)S(1)}, u32[]{:S(2)}, u32[]{:S(2)}) collective-permute-start(f32[8,1024]{1,0:T(8,128)S(1)} %project_kernel.1), channel_id=1, source_target_pairs={{0,1},{1,0},{2,3},{3,2},{4,5},{5,4},{6,7},{7,6},{8,9},{9,8},{10,11... | collective-permute-start | bytes 98312 | tf_op jit(solution)/shard_map/ppermute | solution.py:35
  25.2 4.0 %collective-permute-start.7 = (f32[8,1024]{1,0:T(8,128)S(1)}, f32[8,1024]{1,0:T(8,128)S(1)}, u32[]{:S(2)}, u32[]{:S(2)}) collective-permute-start(f32[8,1024]{1,0:T(8,128)S(1)} %project_kernel.1), channel_id=1, source_target_pairs={{0,2},{1,3},{2,0},{3,1},{4,6},{5,7},{6,4},{7,5},{8,10},{9,11},{10,... | collective-permute-start | bytes 98312 | tf_op jit(solution)/shard_map/ppermute | solution.py:35
  26.7 3.3 %collective-permute-start.8 = (f32[8,1024]{1,0:T(8,128)S(1)}, f32[8,1024]{1,0:T(8,128)S(1)}, u32[]{:S(2)}, u32[]{:S(2)}) collective-permute-start(f32[8,1024]{1,0:T(8,128)S(1)} %project_kernel.1), channel_id=1, source_target_pairs={{0,3},{1,2},{2,1},{3,0},{4,7},{5,6},{6,5},{7,4},{8,11},{9,10},{10,... | collective-permute-start | bytes 98312 | tf_op jit(solution)/shard_map/ppermute | solution.py:35
  30.1 5.1 %collective-permute-start.10 = (bf16[8,1024]{1,0:T(8,128)(2,1)S(1)}, bf16[8,1024]{1,0:T(8,128)(2,1)S(1)}, u32[]{:S(2)}, u32[]{:S(2)}) collective-permute-start(bf16[8,1024]{1,0:T(8,128)(2,1)S(1)} %add_convert_fusion.refs_0_), channel_id=1, source_target_pairs={{0,8},{4,12},{8,0},{12,4},{1,9},{5,13},{9,1},{13,5},{2,10},{6,14},... | collective-permute-start | bytes 49160 | tf_op jit(solution)/shard_map/ppermute | solution.py:35
  30.3 5.5 %collective-permute-start.11 = (bf16[8,1024]{1,0:T(8,128)(2,1)S(1)}, bf16[8,1024]{1,0:T(8,128)(2,1)S(1)}, u32[]{:S(2)}, u32[]{:S(2)}) collective-permute-start(bf16[8,1024]{1,0:T(8,128)(2,1)S(1)} %add_convert_fusion.refs_0_), channel_id=1, source_target_pairs={{0,12},{4,8},{8,4},{12,0},{1,13},{5,9},{9,5},{13,1},{2,14},{6,10},... | collective-permute-start | bytes 49160 | tf_op jit(solution)/shard_map/ppermute | solution.py:35
  33.5 3.7 %collective-permute-start.9 = (bf16[8,1024]{1,0:T(8,128)(2,1)S(1)}, bf16[8,1024]{1,0:T(8,128)(2,1)S(1)}, u32[]{:S(2)}, u32[]{:S(2)}) collective-permute-start(bf16[8,1024]{1,0:T(8,128)(2,1)S(1)} %add_convert_fusion.refs_0_), channel_id=1, source_target_pairs={{0,4},{4,0},{8,12},{12,8},{1,5},{5,1},{9,13},{13,9},{2,6},{6,2},{1... | collective-permute-start | bytes 49160 | tf_op jit(solution)/shard_map/ppermute | solution.py:35
  41.5 11.6 %all-to-all-start = ((f32[16,8,256]{2,1,0:T(8,128)}), f32[16,8,256]{2,1,0:T(8,128)S(1)}, u32[]{:S(2)}, u32[]{:S(2)}) async-start(f32[16,8,256]{2,1,0:T(8,128)} %mixer_kernel.1), calls=%async_computation | async-start | bytes 262144 | tf_op jit(solution)/shard_map/all_to_all | solution.py:256
